TPU v7x, 256 devices: a whole 4x4x8 slice. The times are simulated.
256 devices in a mesh: ep: 128 (over z, y, x), tp: 2 (over core).
Axes of the slice: x: 4, y: 4, z: 8, core: 2. Of those that a mesh axis runs over, the one named last changes fastest.
Arguments:
- tokens: bfloat16 [65536, 2048], P(('ep', 'tp')), may hold values from -6 to 6
- norm_gain: float32 [2048], replicated, may hold values from 0.1 to 1.9
- expert_ids: int32 [65536, 2], P(('ep', 'tp')), may hold values from 0 to 127, all different within a row; in each aligned block of 256 rows (0 to 255, 256 to 511, ...) at most 6 rows name the same one
- route_weights: float32 [65536, 2], P(('ep', 'tp')), may hold values from 0.2 to 1.2
- expert_gate: bfloat16 [128, 2048, 512], P('ep', None, 'tp'), may hold values from -0.125 to 0.125
- expert_up: bfloat16 [128, 2048, 512], P('ep', None, 'tp'), may hold values from -0.125 to 0.125
- expert_down: bfloat16 [128, 512, 2048], P('ep', 'tp'), may hold values from -0.25 to 0.25
- shared_gate: bfloat16 [2048, 512], P(None, 'tp'), may hold values from -0.125 to 0.125
- shared_up: bfloat16 [2048, 512], P(None, 'tp'), may hold values from -0.125 to 0.125
- shared_down: bfloat16 [512, 2048], P('tp'), may hold values from -0.25 to 0.25
Outputs:
- mixed: bfloat16 [65536, 2048], P(('ep', 'tp'))
Inputs may be any that keep to these rules, and one draw needn't show every extreme that they name: `expert_ids`: each token names 2 different experts. Among the tokens of one device (aligned blocks of 256 rows) no expert is named by more than 6 tokens, and in every block some expert is named by exactly 6.
All inputs are finite; a program needn't handle non-finite values.
Results may differ from a plain program's by a relative error of at most 0.0075.
Values may be sent and summed in bfloat16 or wider, within the bound.
A program may use at most 64 MiB of HBM per device.

v0:
```python
import jax
import jax.numpy as jnp
from jax import lax
from jax.sharding import PartitionSpec as P

epsilon = 1e-06


def normalize(tokens, norm_gain):
    values = tokens.astype(jnp.float32)
    factor = lax.rsqrt(jnp.mean(values * values, axis=1, keepdims=True) + epsilon)
    return (values * factor * norm_gain[None, :]).astype(jnp.bfloat16)


def round_term(partial_value):
    return lax.optimization_barrier(partial_value.astype(jnp.bfloat16)).astype(jnp.float32)


def gated_rows(row_block, gate_w, up_w):
    gate_value = jnp.dot(row_block, gate_w, preferred_element_type=jnp.float32)
    up_value = jnp.dot(row_block, up_w, preferred_element_type=jnp.float32)
    return (jax.nn.silu(gate_value) * up_value).astype(jnp.bfloat16)


def sliced_term(hidden, down_w):
    return round_term(jnp.dot(hidden, down_w, preferred_element_type=jnp.float32))


def shared_branch(normed, shared_gate, shared_up, shared_down):
    hidden = gated_rows(lax.all_gather(normed, "tp", axis=0, tiled=True), shared_gate, shared_up)
    return lax.psum_scatter(
        sliced_term(hidden, shared_down).astype(jnp.bfloat16), "tp", scatter_dimension=0, tiled=True
    ).astype(jnp.float32)


def body(
    tokens,
    norm_gain,
    expert_ids,
    route_weights,
    expert_gate,
    expert_up,
    expert_down,
    shared_gate,
    shared_up,
    shared_down,
):
    normed = normalize(tokens, norm_gain)
    tok_rows = tokens.shape[0]
    model_width = tokens.shape[1]
    top_count = expert_ids.shape[1]
    ep_size = lax.axis_size("ep")
    experts = expert_gate.shape[0] * ep_size
    capacity = 3 * tok_rows * top_count // (2 * experts)
    assigned = tok_rows * top_count
    gate_one = expert_gate[0]
    up_one = expert_up[0]
    down_one = expert_down[0]
    flat_ids = expert_ids.reshape(-1)
    onehot = (flat_ids[:, None] == jnp.arange(experts, dtype=jnp.int32)[None, :]).astype(
        jnp.bfloat16
    )
    earlier = (jnp.arange(assigned)[:, None] > jnp.arange(assigned)[None, :]).astype(jnp.bfloat16)
    before_count = jnp.dot(earlier, onehot, preferred_element_type=jnp.float32)
    slot_index = jnp.sum(before_count * onehot.astype(jnp.float32), axis=1).astype(jnp.int32)
    position = flat_ids * capacity + slot_index
    owners = (
        jnp.full((experts * capacity,), tok_rows, jnp.int32)
        .at[position]
        .set(jnp.arange(assigned, dtype=jnp.int32) // top_count)
    )
    padded = jnp.concatenate([normed, jnp.zeros((1, model_width), jnp.bfloat16)], axis=0)
    outgoing = padded[owners].reshape(ep_size, capacity, model_width)
    received = lax.all_to_all(outgoing, "ep", split_axis=0, concat_axis=0, tiled=True)
    hidden = gated_rows(
        lax.all_gather(received.reshape(ep_size * capacity, model_width), "tp", axis=0, tiled=True),
        gate_one,
        up_one,
    )
    summed = lax.psum_scatter(
        sliced_term(hidden, down_one).astype(jnp.bfloat16), "tp", scatter_dimension=0, tiled=True
    )
    returned = lax.all_to_all(
        summed.reshape(ep_size, capacity, model_width),
        "ep",
        split_axis=0,
        concat_axis=0,
        tiled=True,
    )
    gathered = returned.reshape(experts * capacity, model_width)[position]
    routed = jnp.sum(
        gathered.reshape(tok_rows, top_count, model_width).astype(jnp.float32)
        * route_weights[:, :, None],
        axis=1,
    )
    shared_out = shared_branch(normed, shared_gate, shared_up, shared_down)
    return (routed + shared_out).astype(jnp.bfloat16)


def solution(mesh):
    placed = (
        P(("ep", "tp"), None),
        P(),
        P(("ep", "tp"), None),
        P(("ep", "tp"), None),
        P("ep", None, "tp"),
        P("ep", None, "tp"),
        P("ep", "tp", None),
        P(None, "tp"),
        P(None, "tp"),
        P("tp", None),
    )
    return jax.shard_map(
        body, mesh=mesh, in_specs=placed, out_specs=P(("ep", "tp"), None), check_vma=False
    )
```

profile of v0, /device:TPU:1, one launch (start us, length us, event | category | flops | bytes accessed | tf_op | source)
XLA Modules:
  0.0 344.7 jit_solution(12503295927482520006)
XLA Ops:
  6.5 1.0 copy.13
  7.5 0.7 broadcast_multiply_fusion
  8.2 1.5 fusion.1
  10.5 2.4 scatter_custom_fusion
  13.4 4.3 %gather_fusion = bf16[768,2048]{1,0:T(8,128)(2,1)} fusion(bf16[257,2048]{1,0:T(8,128)(2,1)S(1)} %concatenate.3, s32[1024]{0:T(1024)S(1)} %pad_clamp_fusion.1), kind=kCustom, calls=%fused_computation | custom fusion | bytes 6294528 | tf_op jit(solution)/shard_map/gather | solution.py:73
  17.7 6.2 %reshape.59 = bf16[128,6,2048]{2,1,0:T(8,128)(2,1)} reshape(bf16[768,2048]{1,0:T(8,128)(2,1)} %gather_fusion) | data formatting | bytes 6291456 | tf_op jit(solution)/shard_map/reshape | solution.py:73
  23.9 110.2 %all_to_all.10 = bf16[128,6,2048]{2,1,0:T(8,128)(2,1)} all-to-all(bf16[128,6,2048]{2,1,0:T(8,128)(2,1)} %reshape.59), channel_id=1, replica_groups=mesh['ep'=128,'tp'=2] {'ep'}, dimensions={0} | all-to-all | bytes 6291456 | tf_op jit(solution)/shard_map/all_to_all | solution.py:74
  134.1 6.3 %reshape.60 = bf16[768,2048]{1,0:T(8,128)(2,1)} reshape(bf16[128,6,2048]{2,1,0:T(8,128)(2,1)} %all_to_all.10) | data formatting | bytes 6291456 | tf_op jit(solution)/shard_map/reshape | solution.py:76
  140.7 21.2 %all-gather.3.cloned.1.call-done = bf16[1536,2048]{1,0:T(8,128)(2,1)} async-done(((bf16[768,2048]{1,0:T(8,128)(2,1)}), bf16[1536,2048]{1,0:T(8,128)(2,1)}) %all-gather.3.cloned.1.call-update) | async-done | bytes 6291472 | tf_op jit(solution)/shard_map/all_gather | solution.py:76
  161.9 5.8 %fusion.9 = f32[1536,256]{1,0:T(8,128)} fusion(bf16[1536,2048]{1,0:T(8,128)(2,1)} %all-gather.3.cloned.1.call-done, bf16[1,2048,256]{2,1,0:T(8,128)(2,1)S(1)} %copy-done.7), kind=kOutput, calls=%fused_computation.20 | convolution fusion | flops 1610612736 | bytes 8912896 | tf_op jit(solution)/shard_map/dot_general | solution.py:20
  167.7 12.3 %convolution_convert_fusion = bf16[1536,2048]{1,0:T(8,128)(2,1)} fusion(bf16[1536,2048]{1,0:T(8,128)(2,1)} %all-gather.3.cloned.1.call-done, f32[1536,256]{1,0:T(8,128)} %fusion.9, bf16[1,256,2048]{2,1,0:T(8,128)(2,1)S(1)} %copy-done, bf16[1,2048,256]{2,1,0:T(8,128)(2,1)S(1)} %copy-done.8), kind=kOutput, calls=%fused_computation.3 | convolution fusion | flops 3226730496 | bytes 16252928 | tf_op jit(solution)/shard_map/dot_general | solution.py:26
  180.0 0.7 all-gather.5.cloned.1.call-update
  180.7 20.0 %reduce-scatter.3.cloned.1.call-done = bf16[768,2048]{1,0:T(8,128)(2,1)} async-done(((bf16[1536,2048]{1,0:T(8,128)(2,1)}), bf16[768,2048]{1,0:T(8,128)(2,1)}) %reduce-scatter.3.cloned.1.call-update) | async-done | bytes 3145744 | tf_op jit(solution)/shard_map/reduce_scatter | solution.py:80
  200.7 6.2 %reshape.61 = bf16[128,6,2048]{2,1,0:T(8,128)(2,1)} reshape(bf16[768,2048]{1,0:T(8,128)(2,1)} %reduce-scatter.3.cloned.1.call-done) | data formatting | bytes 6291456 | tf_op jit(solution)/shard_map/reshape | solution.py:84
  206.9 14.3 %all-to-all-start.1 = ((bf16[128,6,2048]{2,1,0:T(8,128)(2,1)}), bf16[128,6,2048]{2,1,0:T(8,128)(2,1)}, u32[]{:S(2)}, u32[]{:S(2)}) async-start(bf16[128,6,2048]{2,1,0:T(8,128)(2,1)} %reshape.61), calls=%async_computation.2 | async-start | bytes 8388608 | tf_op jit(solution)/shard_map/all_to_all | solution.py:83
  221.6 3.2 fusion.27
  224.8 5.4 %convolution_convert_fusion.1 = bf16[512,2048]{1,0:T(8,128)(2,1)} fusion(bf16[256,2048]{1,0:T(8,128)(2,1)} %param.19, bf16[512,2048]{1,0:T(8,128)(2,1)S(1)} %copy-done.6, bf16[2048,256]{1,0:T(8,128)(2,1)} %param.18, f32[512,256]{1,0:T(8,128)} %fusion.27), kind=kOutput, calls=%fused_computation.5 | convolution fusion | flops 1075576832 | bytes 6815744 | tf_op jit(solution)/shard_map/dot_general | solution.py:26
  230.2 0.7 copy-done.5
  231.0 82.2 %all-to-all-done.1 = bf16[128,6,2048]{2,1,0:T(8,128)(2,1)} async-done(((bf16[128,6,2048]{2,1,0:T(8,128)(2,1)}), bf16[128,6,2048]{2,1,0:T(8,128)(2,1)}, u32[]{:S(2)}, u32[]{:S(2)}) %all-to-all-start.1) | async-done | bytes 3145760 | tf_op jit(solution)/shard_map/all_to_all | solution.py:83
  313.2 4.9 %reshape.62 = bf16[768,2048]{1,0:T(8,128)(2,1)S(1)} reshape(bf16[128,6,2048]{2,1,0:T(8,128)(2,1)} %all-to-all-done.1) | data formatting | bytes 6291456 | tf_op jit(solution)/shard_map/reshape | solution.py:90
  318.1 3.3 gather_fusion.1
  321.4 5.4 %reshape.63 = f32[256,2,2048]{2,1,0:T(2,128)} reshape(bf16[512,2048]{1,0:T(8,128)(2,1)} %gather_fusion.1) | data formatting | bytes 6291456 | tf_op jit(solution)/shard_map/convert_element_type | solution.py:92
  326.8 8.9 %multiply_reduce_fusion = f32[256,2048]{1,0:T(8,128)S(1)} fusion(f32[256,2,2048]{2,1,0:T(2,128)} %reshape.63, f32[256,2]{1,0:T(8,128)S(1)} %copy.14), kind=kLoop, calls=%fused_computation.4 | loop fusion | flops 1572864 | bytes 6293504 | tf_op jit(solution)/shard_map/reduce_sum | solution.py:91
  335.7 2.5 add_convert_fusion
  (42 shorter events, 2.0 us)
Async XLA Ops:
  6.5 161.1 %copy-start = (bf16[1,256,2048]{2,1,0:T(8,128)(2,1)S(1)}, bf16[1,256,2048]{2,1,0:T(8,128)(2,1)}, u32[]{:S(2)}) copy-start(bf16[1,256,2048]{2,1,0:T(8,128)(2,1)} %param.16) | copy-start | bytes 3145732
  6.5 6.4 %copy-start.3 = (bf16[256,2048]{1,0:T(8,128)(2,1)S(1)}, bf16[256,2048]{1,0:T(8,128)(2,1)}, u32[]{:S(2)}) copy-start(bf16[256,2048]{1,0:T(8,128)(2,1)} %param.10) | copy-start | bytes 3145732
  6.5 6.5 %copy-start.4 = (f32[2048]{0:T(1024)S(1)}, f32[2048]{0:T(1024)}, u32[]{:S(2)}) copy-start(f32[2048]{0:T(1024)} %param.11) | copy-start | bytes 24580
  6.5 155.3 %all-gather.3.cloned.1.call-start = ((), (), s32[]{:S(2)}) async-start(), calls=%async_computation.4 | async-start | bytes 9437184 | tf_op jit(solution)/shard_map/all_gather | solution.py:76
  13.3 4.4 %copy-start.2 = (bf16[256,2048]{1,0:T(8,128)(2,1)}, bf16[256,2048]{1,0:T(8,128)(2,1)S(1)}, u32[]{:S(2)}) copy-start(bf16[256,2048]{1,0:T(8,128)(2,1)S(1)} %fusion.3) | copy-start | bytes 3145732
  140.4 21.4 %copy-start.7 = (bf16[1,2048,256]{2,1,0:T(8,128)(2,1)S(1)}, bf16[1,2048,256]{2,1,0:T(8,128)(2,1)}, u32[]{:S(2)}) copy-start(bf16[1,2048,256]{2,1,0:T(8,128)(2,1)} %param.14) | copy-start | bytes 3145732
  140.5 27.2 %copy-start.8 = (bf16[1,2048,256]{2,1,0:T(8,128)(2,1)S(1)}, bf16[1,2048,256]{2,1,0:T(8,128)(2,1)}, u32[]{:S(2)}) copy-start(bf16[1,2048,256]{2,1,0:T(8,128)(2,1)} %param.15) | copy-start | bytes 3145732
  140.5 60.2 %reduce-scatter.3.cloned.1.call-start = ((), (), s32[]{:S(2)}) async-start(), calls=%async_computation.5 | async-start | bytes 9437184 | tf_op jit(solution)/shard_map/reduce_scatter | solution.py:80
  180.0 41.5 %all-gather.5.cloned.1.call-start = ((), (), s32[]{:S(2)}) async-start(), calls=%async_computation.6 | async-start | bytes 3145728 | tf_op jit(solution)/shard_map/all_gather | solution.py:30
  206.9 14.6 %copy-start.9 = (bf16[2048,256]{1,0:T(8,128)(2,1)S(1)}, bf16[2048,256]{1,0:T(8,128)(2,1)}, u32[]{:S(2)}) copy-start(bf16[2048,256]{1,0:T(8,128)(2,1)} %param.17) | copy-start | bytes 3145732
  206.9 106.2 %all-to-all-start.1 = ((bf16[128,6,2048]{2,1,0:T(8,128)(2,1)}), bf16[128,6,2048]{2,1,0:T(8,128)(2,1)}, u32[]{:S(2)}, u32[]{:S(2)}) async-start(bf16[128,6,2048]{2,1,0:T(8,128)(2,1)} %reshape.61), calls=%async_computation.2 | async-start | bytes 8388608 | tf_op jit(solution)/shard_map/all_to_all | solution.py:83
  221.2 114.5 %reduce-scatter.5.cloned.1.call-start = ((), (), s32[]{:S(2)}) async-start(), calls=%async_computation.7 | async-start | bytes 3145728 | tf_op jit(solution)/shard_map/reduce_scatter | solution.py:31
  221.5 3.3 copy-start.6
  230.2 0.7 copy-start.5
  326.8 11.4 %copy-start.1 = (bf16[1,256,2048]{2,1,0:T(8,128)(2,1)S(1)}, bf16[1,256,2048]{2,1,0:T(8,128)(2,1)}, u32[]{:S(2)}) copy-start(bf16[1,256,2048]{2,1,0:T(8,128)(2,1)} %param.16) | copy-start | bytes 3145732
Sparse Core Ops, SparseCore 0:
  140.6 21.2 all-gather.2
  180.1 20.5 reduce-scatter.2
  202.5 18.1 all-gather.4
  230.3 16.9 reduce-scatter.4
where the time goes:
time: 349 us; the launch traced here: 345 us
  waiting for transfers between devices  124 us (36%)
  blocking collectives  110 us (32%)
  local copies, waits for them, and re-layouts  41.4 us (12%)
  matrix products  27 us (8%)
  starting transfers between devices  14.8 us (4%)
  other arithmetic  13.9 us (4%)
  between operations  13.3 us (4%)
    all_to_all x1, blocking collectives, body(): lax.all_to_all(outgoing, 'ep', split_axis=0, concat_axis=0, tiled=True)  110 us
    all_to_all x1, waiting for transfers between devices, body(): lax.all_to_all(summed.reshape(ep_size, capacity, model_width), 'ep', spli...  82.2 us
    all_gather x1, waiting for transfers between devices, body(): lax.all_gather(received.reshape(ep_size * capacity, model_width), 'tp', a...  21.2 us
    reduce_scatter x1, waiting for transfers between devices, body(): lax.psum_scatter(sliced_term(hidden, down_one).astype(jnp.bfloat16), 'tp'...  20 us
    dot_general x2, matrix products, sliced_term(): jnp.dot(hidden, down_w, preferred_element_type=jnp.float32)  17.7 us
    all_to_all x1, starting transfers between devices, body(): lax.all_to_all(summed.reshape(ep_size, capacity, model_width), 'ep', spli...  14.3 us
    dot_general x2, matrix products, gated_rows(): gate_value = jnp.dot(row_block, gate_w, preferred_element_type=jnp.float32)  9.01 us
    reduce_sum x1, other arithmetic, body(): jnp.sum(gathered.reshape(tok_rows, top_count, model_width).astype(jnp.flo...  8.86 us
  transfers between devices with their start and end apart: 5, of which 3 were waited for; matrix products, arithmetic and copies ran while one was open for 11% of the time, Pallas kernels for 0%

commit v1 on v0

v1 whole, which is shorter than its diff:
```python
import functools

import jax
import jax.numpy as jnp
from jax import lax
from jax.experimental import pallas as pl
from jax.experimental.pallas import tpu as pltpu
from jax.sharding import PartitionSpec as P

MESH = pl.DeviceIdType.MESH
F32, BF16 = jnp.float32, jnp.bfloat16
epsilon = 1e-06
LANES, SUB = 128, 16
NZ, NY, NX = 8, 4, 4


def kernel(
    tokens_ref, gain_ref, ids_ref, weights_ref, eg_ref, eu_ref, ed_ref, sg_ref, su_ref, sd_ref,
    out_ref,
    normed, outgoing, received, results, returned, stage, rows, total, pcol, prow,
    wg, wu, wd, vg, vu, vd,
    local_sem, half_send, half_recv, out_send, out_recv, back_send, back_recv,
):
    plane = NY * NX
    experts = NZ * plane
    tok = tokens_ref.shape[0]
    capacity = received.shape[1] // SUB
    many = plane * capacity
    me, core = lax.axis_index("ep"), lax.axis_index("tp")
    z, y, x = me // plane, (me // NX) % NY, me % NX

    def at(dz, dy, dx):
        return ((z + dz) % NZ) * plane + ((y + dy) % NY) * NX + (x + dx) % NX

    barrier = pltpu.get_barrier_semaphore()

    def greet(step, carry):
        there = at(step // plane, (step // NX) % NY, step % NX)
        pl.semaphore_signal(barrier, inc=1, device_id=(there, core), device_id_type=MESH)
        return carry

    lax.fori_loop(1, experts, greet, 0)
    pl.semaphore_signal(barrier, inc=1, device_id=(me, 1 - core), device_id_type=MESH)

    pairs = (
        (sg_ref, vg), (su_ref, vu), (sd_ref, vd), (eg_ref.at[0], wg), (eu_ref.at[0], wu), (ed_ref.at[0], wd),
    )
    own = [pltpu.make_async_copy(a, b.at[0], local_sem.at[i]) for i, (a, b) in enumerate(pairs)]
    other = [
        pltpu.make_async_remote_copy(
            src_ref=a, dst_ref=b.at[1], send_sem=half_send.at[i], recv_sem=half_recv.at[i],
            device_id=(me, 1 - core), device_id_type=MESH,
        )
        for i, (a, b) in enumerate(pairs)
    ]
    for copy in own:
        copy.start()

    values = tokens_ref[...].astype(F32)
    factor = lax.rsqrt(jnp.mean(values * values, axis=1, keepdims=True) + epsilon)
    normed[...] = (values * factor * gain_ref[...]).astype(BF16)

    expert_at = lax.broadcasted_iota(jnp.int32, (tok, experts), 1)
    lower = (
        lax.broadcasted_iota(jnp.int32, (tok, tok), 0) > lax.broadcasted_iota(jnp.int32, (tok, tok), 1)
    ).astype(BF16)
    base = jnp.zeros((1, experts), F32)
    for j in range(2):
        named = ids_ref[:, j : j + 1]
        hot = (named == expert_at).astype(F32)
        before = jnp.dot(lower, hot.astype(BF16), preferred_element_type=F32) + base
        slot = jnp.sum(hot * before, axis=1, keepdims=True)
        base = base + jnp.sum(hot, axis=0, keepdims=True)
        position = jnp.broadcast_to(named.astype(F32) * capacity + slot, (tok, LANES))
        pcol[j] = position.astype(jnp.int32)
        prow[j] = jnp.transpose(position)[0:8].astype(jnp.int32)

    pl.semaphore_wait(barrier, experts)

    def turn(step):
        odd = step % 2
        return odd * ((step + 1) // 2) + (1 - odd) * ((NZ - step // 2) % NZ)

    def to_rows(source, first):
        flat = source[pl.ds(first, plane)].reshape(many * SUB, LANES)
        stage[...] = flat.astype(F32)
        for c in range(SUB):
            rows[:, c * LANES : (c + 1) * LANES] = stage[pl.ds(c, many, stride=SUB), :].astype(BF16)

    def from_block(block, c, width):
        for k in range(width // LANES):
            stage[pl.ds(c * (width // LANES) + k, many, stride=SUB), :] = block[:, k * LANES : (k + 1) * LANES]

    def to_flat(target, first):
        target[pl.ds(first, plane)] = stage[...].astype(BF16).reshape(plane, capacity * SUB, LANES)

    def dispatch(step, carry):
        dz = turn(step)
        zt = (z + dz) % NZ
        slots = lax.broadcasted_iota(jnp.int32, (many, tok), 0) + zt * many
        pick = ((slots == prow[0, 0:1]) | (slots == prow[1, 0:1])).astype(BF16)
        width = 256
        for c in range(SUB * LANES // width):
            from_block(
                jnp.dot(pick, normed[:, c * width : (c + 1) * width], preferred_element_type=F32), c, width
            )
        to_flat(outgoing, zt * plane)

        def send(i, carry):
            there = at(dz, i // NX, i % NX)
            pltpu.make_async_remote_copy(
                src_ref=outgoing.at[there], dst_ref=received.at[me], send_sem=out_send,
                recv_sem=out_recv.at[dz], device_id=(there, core), device_id_type=MESH,
            ).start()
            return carry

        @pl.when(step == 0)
        def _():
            pltpu.make_async_copy(outgoing.at[me], received.at[me], out_recv.at[0]).start()

        lax.fori_loop(jnp.where(step == 0, 1, 0), plane, send, 0)
        return carry

    lax.fori_loop(0, NZ, dispatch, 0)
    for copy in other:
        copy.start()

    def gated(block, gate_w, up_w):
        parts = []
        for h in range(2):
            gate = jnp.dot(block, gate_w[h], preferred_element_type=F32)
            up = jnp.dot(block, up_w[h], preferred_element_type=F32)
            parts.append((gate / (1.0 + jnp.exp(-gate)) * up).astype(BF16))
        return parts

    def down(parts, down_w, c, width):
        return sum(
            jnp.dot(parts[h], down_w[h, :, c * width : (c + 1) * width], preferred_element_type=F32)
            for h in range(2)
        )

    for i in range(3):
        own[i].wait()
        other[i].wait()
    step_rows = tok // 2

    def shared(step, carry):
        at_rows = pl.ds(pl.multiple_of(step * step_rows, step_rows), step_rows)
        parts = gated(normed[at_rows, :], vg, vu)
        for c in range(4):
            total[at_rows, c * 512 : (c + 1) * 512] = down(parts, vd, c, 512)
        return carry

    lax.fori_loop(0, 2, shared, 0)
    for i in range(3, 6):
        own[i].wait()
        other[i].wait()

    def expert(step, carry):
        dz = turn(step)
        zs = (z + NZ - dz) % NZ
        pltpu.make_async_remote_copy(
            src_ref=outgoing.at[pl.ds(0, plane)], dst_ref=received.at[pl.ds(zs * plane, plane)],
            send_sem=out_send, recv_sem=out_recv.at[dz], device_id=(me, 1 - core), device_id_type=MESH,
        ).wait_recv()
        to_rows(received, zs * plane)
        parts = gated(rows[...], wg, wu)
        for c in range(4):
            from_block(down(parts, wd, c, 512), c, 512)
        to_flat(results, zs * plane)

        def send(i, carry):
            there = at(NZ - dz, i // NX, i % NX)
            pltpu.make_async_remote_copy(
                src_ref=results.at[there], dst_ref=returned.at[me], send_sem=back_send,
                recv_sem=back_recv.at[dz], device_id=(there, core), device_id_type=MESH,
            ).start()
            return carry

        @pl.when(step == 0)
        def _():
            pltpu.make_async_copy(results.at[me], returned.at[me], back_recv.at[0]).start()

        lax.fori_loop(jnp.where(step == 0, 1, 0), plane, send, 0)
        return carry

    lax.fori_loop(0, NZ, expert, 0)

    def combine(step, carry):
        dz = turn(step)
        zt = (z + dz) % NZ
        pltpu.make_async_remote_copy(
            src_ref=results.at[pl.ds(0, plane)], dst_ref=returned.at[pl.ds(zt * plane, plane)],
            send_sem=back_send, recv_sem=back_recv.at[dz], device_id=(me, 1 - core), device_id_type=MESH,
        ).wait_recv()
        to_rows(returned, zt * plane)
        slots = lax.broadcasted_iota(jnp.int32, (tok, many), 1) + zt * many
        share = jnp.zeros((tok, many), F32)
        for j in range(2):
            share = share + jnp.where(slots == pcol[j, :, 0:1], weights_ref[:, j : j + 1], 0.0)
        high = share.astype(BF16)
        low = (share - high.astype(F32)).astype(BF16)
        for c in range(4):
            part = rows[:, c * 512 : (c + 1) * 512]
            total[:, c * 512 : (c + 1) * 512] += jnp.dot(
                high, part, preferred_element_type=F32
            ) + jnp.dot(low, part, preferred_element_type=F32)
        return carry

    lax.fori_loop(0, NZ, combine, 0)
    out_ref[...] = total[...].astype(BF16)

    pltpu.make_async_remote_copy(
        src_ref=outgoing.at[pl.ds(0, experts - 1)], dst_ref=received.at[pl.ds(0, experts - 1)],
        send_sem=out_send, recv_sem=out_recv.at[0], device_id=(me, 1 - core), device_id_type=MESH,
    ).wait_send()
    pltpu.make_async_remote_copy(
        src_ref=results.at[pl.ds(0, experts - 1)], dst_ref=returned.at[pl.ds(0, experts - 1)],
        send_sem=back_send, recv_sem=back_recv.at[0], device_id=(me, 1 - core), device_id_type=MESH,
    ).wait_send()


def body(tokens, norm_gain, expert_ids, route_weights, eg, eu, ed, sg, su, sd):
    tok, width = tokens.shape
    experts = eg.shape[0] * lax.axis_size("ep")
    capacity = 3 * tok * expert_ids.shape[1] // (2 * experts)
    many = NY * NX * capacity
    half, half_shared = eg.shape[2], sg.shape[1]
    slots = pltpu.VMEM((experts, capacity * SUB, LANES), BF16)
    vmem, hbm = pl.BlockSpec(memory_space=pltpu.VMEM), pl.BlockSpec(memory_space=pl.ANY)
    dma = pltpu.SemaphoreType.DMA
    return pl.pallas_call(
        kernel,
        out_shape=jax.ShapeDtypeStruct((tok, width), BF16),
        in_specs=[vmem] * 4 + [hbm] * 6,
        out_specs=vmem,
        scratch_shapes=[
            pltpu.VMEM((tok, width), BF16),
            slots, slots, slots, slots,
            pltpu.VMEM((many * SUB, LANES), F32),
            pltpu.VMEM((many, width), BF16),
            pltpu.VMEM((tok, width), F32),
            pltpu.VMEM((2, tok, LANES), jnp.int32),
            pltpu.VMEM((2, 8, tok), jnp.int32),
            pltpu.VMEM((2, width, half), BF16), pltpu.VMEM((2, width, half), BF16), pltpu.VMEM((2, half, width), BF16),
            pltpu.VMEM((2, width, half_shared), BF16), pltpu.VMEM((2, width, half_shared), BF16),
            pltpu.VMEM((2, half_shared, width), BF16),
            dma((6,)), dma((6,)), dma((6,)), dma, dma((NZ,)), dma, dma((NZ,)),
        ],
        compiler_params=pltpu.CompilerParams(
            collective_id=0, has_side_effects=True, vmem_limit_bytes=60 * 2**20
        ),
        name="moe",
    )(tokens, norm_gain.reshape(1, width), expert_ids, route_weights, eg, eu, ed, sg, su, sd)


def solution(mesh):
    placed = (
        P(("ep", "tp"), None),
        P(),
        P(("ep", "tp"), None),
        P(("ep", "tp"), None),
        P("ep", None, "tp"),
        P("ep", None, "tp"),
        P("ep", "tp", None),
        P(None, "tp"),
        P(None, "tp"),
        P("tp", None),
    )
    return jax.shard_map(
        body, mesh=mesh, in_specs=placed, out_specs=P(("ep", "tp"), None), check_vma=False
    )
```

time: 349 us -> 162 us (0.46)
  the two profiles are of different devices: /device:TPU:1 before, /device:TPU:32 now
where the time goes in v1:
time: 162 us
  Pallas kernels  157 us (97%)
  local copies, waits for them, and re-layouts  4.59 us (3%)
    pallas_call x1, Pallas kernels, body(): pl.pallas_call(kernel, out_shape=jax.ShapeDtypeStruct((tok, width), BF16)...  157 us
    unnamed x5, local copies, waits for them, and re-layouts  4.59 us

profile of v1, /device:TPU:32, one launch (start us, length us, event | category | flops | bytes accessed | tf_op | source)
XLA Modules:
  0.0 161.8 jit_solution(14728002180875245689)
XLA Ops:
  0.0 0.0 copy-start
  0.0 1.5 copy.11.ids_ref
  1.5 0.0 copy-done
  1.5 0.8 copy.12.weights_ref
  2.3 157.2 %moe.1 = bf16[256,2048]{1,0:T(8,128)(2,1)} custom-call(bf16[256,2048]{1,0:T(8,128)(2,1)} %tokens_ref.1, f32[1,2048]{1,0:T(1,128)} %bitcast.1, s32[256,2]{1,0:T(8,128)} %copy.11.ids_ref, f32[256,2]{1,0:T(8,128)} %copy.12.weights_ref, bf16[1,2048,256]{2,1,0:T(8,128)(2,1)} %eg_ref.1, bf16[1,2048,256]{2,1,0:T(8,128)(2,1)} %eu_ref.1, ...), custom_call_target="tpu_custom_call" | custom-call | tf_op jit(solution)/shard_map/moe/pallas_call | solution.py:232
  159.5 2.3 %copy.14 = bf16[256,2048]{1,0:T(8,128)(2,1)} copy(bf16[256,2048]{1,0:T(8,128)(2,1)} %moe.1) | data formatting | bytes 2097152
Async XLA Ops:
  0.0 1.5 copy-start

commit v2 on v1

v2 whole, which is shorter than its diff:
```python
import jax
import jax.numpy as jnp
from jax import lax
from jax.experimental import pallas as pl
from jax.experimental.pallas import tpu as pltpu
from jax.sharding import PartitionSpec as P

MESH = pl.DeviceIdType.MESH
F32, BF16 = jnp.float32, jnp.bfloat16
epsilon = 1e-06
LANES, SUB = 128, 16
NZ, NY, NX = 8, 4, 4


def kernel(
    tokens_hbm, gain_ref, ids_ref, weights_ref, eg_ref, eu_ref, ed_ref, sg_ref, su_ref, sd_ref,
    out_ref,
    tokens_ref, normed, outgoing, received, results, returned, stage, rows, total, pcol, wcol, prow,
    wg, wu, wd, vg, vu, vd,
    token_sem, ready, local_sem, half_send, half_recv, out_send, out_recv, back_send, back_recv,
):
    plane = NY * NX
    experts = NZ * plane
    groups, group = plane // 2, 2 * NZ
    tok = tokens_ref.shape[0]
    capacity = received.shape[1] // SUB
    many = group * capacity
    me, core = lax.axis_index("ep"), lax.axis_index("tp")
    z, q = me // plane, me % plane
    place = q * NZ + z
    way = 1 - 2 * core

    load = pltpu.make_async_copy(tokens_hbm, tokens_ref, token_sem)
    load.start()

    def turn(step):
        odd = step % 2
        return odd * ((step + 1) // 2) + (1 - odd) * ((NZ - step // 2) % NZ)

    def ahead(step):
        return (z + way * turn(step) + NZ) % NZ

    def partner(step):
        pair, value, bit = q // 2, 0, 1
        while bit < groups:
            value = value + bit * ((pair // bit + step // bit) % 2)
            bit *= 2
        return value

    def member(step, i):
        there_q = 2 * partner(step) + (q + i // NZ) % 2
        there_z = ahead(i % NZ)
        return there_q * NZ + there_z, there_z * plane + there_q

    def first(step):
        return jnp.where(step == 0, 1, 0)

    barrier = pltpu.get_barrier_semaphore()

    def greet_along(i, carry):
        there = ahead(NZ - i) * plane + q
        pl.semaphore_signal(barrier, inc=1, device_id=(there, core), device_id_type=MESH)
        return carry

    def greet_across(semaphore):
        def greet(i, carry):
            there = z * plane + (q + i) % plane
            pl.semaphore_signal(semaphore, inc=1, device_id=(there, core), device_id_type=MESH)
            return carry

        lax.fori_loop(1, plane, greet, 0)

    lax.fori_loop(1, NZ, greet_along, 0)
    greet_across(barrier)
    pl.semaphore_signal(barrier, inc=1, device_id=(me, 1 - core), device_id_type=MESH)

    pairs = (
        (eg_ref.at[0], wg), (eu_ref.at[0], wu), (ed_ref.at[0], wd), (sg_ref, vg), (su_ref, vu), (sd_ref, vd),
    )
    own = [pltpu.make_async_copy(a, b.at[0], local_sem.at[i]) for i, (a, b) in enumerate(pairs)]
    other = [
        pltpu.make_async_remote_copy(
            src_ref=a, dst_ref=b.at[1], send_sem=half_send.at[i], recv_sem=half_recv.at[i],
            device_id=(me, 1 - core), device_id_type=MESH,
        )
        for i, (a, b) in enumerate(pairs)
    ]
    for copy in own:
        copy.start()

    expert_at = lax.broadcasted_iota(jnp.int32, (experts, tok), 0).astype(F32)
    earlier = (
        lax.broadcasted_iota(jnp.int32, (tok, tok), 0) < lax.broadcasted_iota(jnp.int32, (tok, tok), 1)
    ).astype(BF16)
    base = jnp.zeros((experts, 1), F32)
    for j in range(2):
        named = ids_ref[j : j + 1, :].astype(F32)
        high = jnp.floor(named * (1.0 / plane))
        named = (named - high * plane) * NZ + high
        hot = (named == expert_at).astype(F32)
        before = jnp.dot(hot.astype(BF16), earlier, preferred_element_type=F32) + base
        slot = jnp.sum(hot * before, axis=0, keepdims=True)
        base = base + jnp.sum(hot, axis=1, keepdims=True)
        prow[j : j + 1, :] = named * capacity + slot

    pl.semaphore_wait(barrier, NZ - 1 + plane - 1 + 1)
    greet_across(ready)
    load.wait()

    def from_block(block, c, width):
        for k in range(width // LANES):
            stage[pl.ds(c * (width // LANES) + k, many, stride=SUB), :] = block[:, k * LANES : (k + 1) * LANES]

    def to_flat(target, start):
        target[pl.ds(start, group)] = stage[...].astype(BF16).reshape(group, capacity * SUB, LANES)

    def from_flat(source, start):
        stage[...] = source[pl.ds(start, group)].reshape(many * SUB, LANES).astype(F32)

    def column(c):
        return stage[pl.ds(c, many, stride=SUB), :]

    def dispatch(step, carry):
        start = partner(step) * group
        slots = (lax.broadcasted_iota(jnp.int32, (many, tok), 0) + start * capacity).astype(F32)
        pick = ((slots == prow[0:1, :]) | (slots == prow[1:2, :])).astype(BF16)
        width = 256
        for c in range(SUB * LANES // width):
            from_block(
                jnp.dot(pick, tokens_ref[:, c * width : (c + 1) * width], preferred_element_type=F32), c, width
            )
        to_flat(outgoing, start)

        def send(i, carry):
            slot, there = member(step, i)
            pltpu.make_async_remote_copy(
                src_ref=outgoing.at[slot], dst_ref=received.at[place], send_sem=out_send,
                recv_sem=out_recv.at[step], device_id=(there, core), device_id_type=MESH,
            ).start()
            return carry

        @pl.when(step == 0)
        def _():
            pltpu.make_async_copy(outgoing.at[place], received.at[place], out_recv.at[0]).start()

        lax.fori_loop(first(step), NZ, send, 0)

        @pl.when(step == 0)
        def _():
            pl.semaphore_wait(ready, plane - 1)

        lax.fori_loop(NZ, group, send, 0)
        return carry

    lax.fori_loop(0, groups, dispatch, 0)
    for copy in other:
        copy.start()

    for j in range(2):
        pcol[j] = jnp.transpose(jnp.broadcast_to(prow[j : j + 1, :], (LANES, tok)))
        wcol[j] = jnp.transpose(jnp.broadcast_to(weights_ref[j : j + 1, :], (LANES, tok)))

    def gated(block, gate_w, up_w):
        parts = []
        for h in range(2):
            gate = jnp.dot(block, gate_w[h], preferred_element_type=F32)
            up = jnp.dot(block, up_w[h], preferred_element_type=F32)
            parts.append((gate / (1.0 + jnp.exp(-gate)) * up).astype(BF16))
        return parts

    def down(parts, down_w, c, width):
        return sum(
            jnp.dot(parts[h], down_w[h, :, c * width : (c + 1) * width], preferred_element_type=F32)
            for h in range(2)
        )

    for i in range(3):
        own[i].wait()
        other[i].wait()

    def expert(step, carry):
        start = partner(step) * group
        pltpu.make_async_remote_copy(
            src_ref=outgoing.at[pl.ds(0, group)], dst_ref=received.at[pl.ds(start, group)],
            send_sem=out_send, recv_sem=out_recv.at[step], device_id=(me, 1 - core), device_id_type=MESH,
        ).wait_recv()
        from_flat(received, start)
        squares = jnp.zeros((many, LANES), F32)
        for c in range(SUB):
            squares = squares + column(c) * column(c)
        mean = jnp.sum(squares, axis=1, keepdims=True) * (1.0 / (SUB * LANES))
        factor = lax.rsqrt(mean + epsilon)
        for c in range(SUB):
            lanes = slice(c * LANES, (c + 1) * LANES)
            rows[:, lanes] = (column(c) * factor * gain_ref[:, lanes]).astype(BF16)
        parts = gated(rows[...], wg, wu)
        for c in range(4):
            from_block(down(parts, wd, c, 512), c, 512)
        to_flat(results, start)

        def send(i, carry):
            slot, there = member(step, i)
            pltpu.make_async_remote_copy(
                src_ref=results.at[slot], dst_ref=returned.at[place], send_sem=back_send,
                recv_sem=back_recv.at[step], device_id=(there, core), device_id_type=MESH,
            ).start()
            return carry

        @pl.when(step == 0)
        def _():
            pltpu.make_async_copy(results.at[place], returned.at[place], back_recv.at[0]).start()

        lax.fori_loop(first(step), group, send, 0)
        return carry

    lax.fori_loop(0, groups, expert, 0)

    values = tokens_ref[...].astype(F32)
    scale = lax.rsqrt(jnp.mean(values * values, axis=1, keepdims=True) + epsilon)
    normed[...] = (values * scale * gain_ref[...]).astype(BF16)
    for i in range(3, 6):
        own[i].wait()
        other[i].wait()
    step_rows = tok // 2

    def shared(step, carry):
        at_rows = pl.ds(pl.multiple_of(step * step_rows, step_rows), step_rows)
        parts = gated(normed[at_rows, :], vg, vu)
        for c in range(4):
            total[at_rows, c * 512 : (c + 1) * 512] = down(parts, vd, c, 512)
        return carry

    lax.fori_loop(0, 2, shared, 0)

    def combine(step, carry):
        start = partner(step) * group
        slots = (lax.broadcasted_iota(jnp.int32, (tok, many), 1) + start * capacity).astype(F32)
        share = jnp.zeros((tok, many), F32)
        for j in range(2):
            share = share + jnp.where(slots == pcol[j, :, 0:1], wcol[j, :, 0:1], 0.0)
        high = share.astype(BF16)
        low = (share - high.astype(F32)).astype(BF16)
        pltpu.make_async_remote_copy(
            src_ref=results.at[pl.ds(0, group)], dst_ref=returned.at[pl.ds(start, group)],
            send_sem=back_send, recv_sem=back_recv.at[step], device_id=(me, 1 - core), device_id_type=MESH,
        ).wait_recv()
        from_flat(returned, start)
        for c in range(SUB):
            rows[:, c * LANES : (c + 1) * LANES] = column(c).astype(BF16)
        for c in range(4):
            part = rows[:, c * 512 : (c + 1) * 512]
            total[:, c * 512 : (c + 1) * 512] += jnp.dot(
                high, part, preferred_element_type=F32
            ) + jnp.dot(low, part, preferred_element_type=F32)
        return carry

    lax.fori_loop(0, groups, combine, 0)
    out_ref[...] = total[...].astype(BF16)

    pltpu.make_async_remote_copy(
        src_ref=outgoing.at[pl.ds(0, experts - 1)], dst_ref=received.at[pl.ds(0, experts - 1)],
        send_sem=out_send, recv_sem=out_recv.at[0], device_id=(me, 1 - core), device_id_type=MESH,
    ).wait_send()
    pltpu.make_async_remote_copy(
        src_ref=results.at[pl.ds(0, experts - 1)], dst_ref=returned.at[pl.ds(0, experts - 1)],
        send_sem=back_send, recv_sem=back_recv.at[0], device_id=(me, 1 - core), device_id_type=MESH,
    ).wait_send()


def body(tokens, norm_gain, expert_ids, route_weights, eg, eu, ed, sg, su, sd):
    tok, width = tokens.shape
    experts = eg.shape[0] * lax.axis_size("ep")
    capacity = 3 * tok * expert_ids.shape[1] // (2 * experts)
    many = 2 * NZ * capacity
    half, half_shared = eg.shape[2], sg.shape[1]
    slots = pltpu.VMEM((experts, capacity * SUB, LANES), BF16)
    vmem, hbm = pl.BlockSpec(memory_space=pltpu.VMEM), pl.BlockSpec(memory_space=pltpu.HBM)
    dma = pltpu.SemaphoreType.DMA

    def stay(array):
        return pltpu.with_memory_space_constraint(array, pltpu.HBM)

    return pl.pallas_call(
        kernel,
        out_shape=jax.ShapeDtypeStruct((tok, width), BF16),
        in_specs=[hbm] + [vmem] * 3 + [hbm] * 6,
        out_specs=vmem,
        scratch_shapes=[
            pltpu.VMEM((tok, width), BF16), pltpu.VMEM((tok, width), BF16),
            slots, slots, slots, slots,
            pltpu.VMEM((many * SUB, LANES), F32),
            pltpu.VMEM((many, width), BF16),
            pltpu.VMEM((tok, width), F32),
            pltpu.VMEM((2, tok, LANES), F32), pltpu.VMEM((2, tok, LANES), F32), pltpu.VMEM((8, tok), F32),
            pltpu.VMEM((2, width, half), BF16), pltpu.VMEM((2, width, half), BF16), pltpu.VMEM((2, half, width), BF16),
            pltpu.VMEM((2, width, half_shared), BF16), pltpu.VMEM((2, width, half_shared), BF16),
            pltpu.VMEM((2, half_shared, width), BF16),
            dma, pltpu.SemaphoreType.REGULAR, dma((6,)), dma((6,)), dma((6,)), dma, dma((NY * NX // 2,)), dma, dma((NY * NX // 2,)),
        ],
        compiler_params=pltpu.CompilerParams(
            collective_id=0, has_side_effects=True, vmem_limit_bytes=36 * 2**20
        ),
        name="moe",
    )(
        stay(tokens), stay(norm_gain.reshape(1, width)), stay(expert_ids.T), stay(route_weights.T),
        stay(eg), stay(eu), stay(ed), stay(sg), stay(su), stay(sd),
    )


def solution(mesh):
    placed = (
        P(("ep", "tp"), None),
        P(),
        P(("ep", "tp"), None),
        P(("ep", "tp"), None),
        P("ep", None, "tp"),
        P("ep", None, "tp"),
        P("ep", "tp", None),
        P(None, "tp"),
        P(None, "tp"),
        P("tp", None),
    )
    return jax.shard_map(
        body, mesh=mesh, in_specs=placed, out_specs=P(("ep", "tp"), None), check_vma=False
    )
```

time: 162 us -> 152 us (0.938)
  the two profiles are of different devices: /device:TPU:32 before, /device:TPU:1 now
where the time goes in v2:
time: 152 us; the launch traced here: 151 us
  Pallas kernels  150 us (99%)
    pallas_call x1, Pallas kernels, body(): pl.pallas_call(kernel, out_shape=jax.ShapeDtypeStruct((tok, width), BF16)...  150 us

profile of v2, /device:TPU:1, one launch (start us, length us, event | category | flops | bytes accessed | tf_op | source)
XLA Modules:
  0.0 150.9 jit_solution(2927377705842138983)
XLA Ops:
  0.0 150.0 %moe.1 = bf16[256,2048]{1,0:T(8,128)(2,1)S(1)} custom-call(bf16[256,2048]{1,0:T(8,128)(2,1)} %tokens_hbm.1, f32[1,2048]{1,0:T(1,128)} %bitcast.3, s32[2,256]{1,0:T(2,128)} %bitcast.4, f32[2,256]{1,0:T(2,128)} %bitcast.5, bf16[1,2048,256]{2,1,0:T(8,128)(2,1)} %eg_ref.1, bf16[1,2048,256]{2,1,0:T(8,128)(2,1)} %eu_ref.1, bf16[1,256,2048]{2,1,0:T(8,128)(2,1)} %ed_ref.1, ...), custom_call_target="tpu_custom_call" | custom-call | tf_op jit(solution)/shard_map/moe/pallas_call | solution.py:283
  150.0 1.0 copy.12

commit v3 on v2

--- a/solution.py
+++ b/solution.py
@@ -15,60 +15,52 @@
 def kernel(
     tokens_hbm, gain_ref, ids_ref, weights_ref, eg_ref, eu_ref, ed_ref, sg_ref, su_ref, sd_ref,
     out_ref,
-    tokens_ref, normed, outgoing, received, results, returned, stage, rows, total, pcol, wcol, prow,
+    near, normed, outgoing, received, results, returned, stage, rows, total, pcol, wcol, slots_of,
     wg, wu, wd, vg, vu, vd,
-    token_sem, ready, local_sem, half_send, half_recv, out_send, out_recv, back_send, back_recv,
+    token_sem, ready, near_send, near_recv, local_sem, half_send, half_recv, out_send, out_recv, back_send, back_recv,
 ):
-    plane = NY * NX
-    experts = NZ * plane
-    groups, group = plane // 2, 2 * NZ
-    tok = tokens_ref.shape[0]
+    group = NY * NX
+    experts = NZ * group
+    side = NZ // 2
+    tok = near.shape[1]
     capacity = received.shape[1] // SUB
     many = group * capacity
     me, core = lax.axis_index("ep"), lax.axis_index("tp")
-    z, q = me // plane, me % plane
-    place = q * NZ + z
+    z, y, x = me // group, (me // NX) % NY, me % NX
+    q = me % group
     way = 1 - 2 * core
 
-    load = pltpu.make_async_copy(tokens_hbm, tokens_ref, token_sem)
+    load = pltpu.make_async_copy(tokens_hbm, near.at[0], token_sem)
     load.start()
 
-    def turn(step):
-        odd = step % 2
-        return odd * ((step + 1) // 2) + (1 - odd) * ((NZ - step // 2) % NZ)
-
-    def ahead(step):
-        return (z + way * turn(step) + NZ) % NZ
-
-    def partner(step):
-        pair, value, bit = q // 2, 0, 1
-        while bit < groups:
-            value = value + bit * ((pair // bit + step // bit) % 2)
-            bit *= 2
-        return value
-
-    def member(step, i):
-        there_q = 2 * partner(step) + (q + i // NZ) % 2
-        there_z = ahead(i % NZ)
-        return there_q * NZ + there_z, there_z * plane + there_q
-
-    def first(step):
-        return jnp.where(step == 0, 1, 0)
+    def along(distance):
+        return (z + distance + NZ) % NZ
+
+    def offset(step):
+        return jnp.where(step > side, side - step, step)
+
+    def across(i, sign):
+        there_y = (y + sign * (i // NX) + NY) % NY
+        there_x = (x + sign * (i % NX) + NX) % NX
+        return there_y * NX + there_x
+
+    def first(own):
+        return jnp.where(own, 1, 0)
 
     barrier = pltpu.get_barrier_semaphore()
 
     def greet_along(i, carry):
-        there = ahead(NZ - i) * plane + q
+        there = along(i) * group + q
         pl.semaphore_signal(barrier, inc=1, device_id=(there, core), device_id_type=MESH)
         return carry
 
     def greet_across(semaphore):
         def greet(i, carry):
-            there = z * plane + (q + i) % plane
+            there = z * group + across(i, 1)
             pl.semaphore_signal(semaphore, inc=1, device_id=(there, core), device_id_type=MESH)
             return carry
 
-        lax.fori_loop(1, plane, greet, 0)
+        lax.fori_loop(1, group, greet, 0)
 
     lax.fori_loop(1, NZ, greet_along, 0)
     greet_across(barrier)
@@ -95,17 +87,29 @@
     base = jnp.zeros((experts, 1), F32)
     for j in range(2):
         named = ids_ref[j : j + 1, :].astype(F32)
-        high = jnp.floor(named * (1.0 / plane))
-        named = (named - high * plane) * NZ + high
         hot = (named == expert_at).astype(F32)
         before = jnp.dot(hot.astype(BF16), earlier, preferred_element_type=F32) + base
         slot = jnp.sum(hot * before, axis=0, keepdims=True)
         base = base + jnp.sum(hot, axis=1, keepdims=True)
-        prow[j : j + 1, :] = named * capacity + slot
-
-    pl.semaphore_wait(barrier, NZ - 1 + plane - 1 + 1)
+        slots_of[0, j : j + 1, :] = named * capacity + slot
+
+    load.wait()
+    pl.semaphore_wait(barrier, NZ - 1 + group - 1 + 1)
+
+    def whole(path):
+        there = along(way * (1 - 2 * path)) * group + q
+        return [
+            pltpu.make_async_remote_copy(
+                src_ref=ref.at[0], dst_ref=ref.at[1 + path], send_sem=near_send.at[path, i],
+                recv_sem=near_recv.at[path, i], device_id=(there, core), device_id_type=MESH,
+            )
+            for i, ref in enumerate((near, slots_of))
+        ]
+
+    ahead, behind = whole(0), whole(1)
+    for copy in ahead:
+        copy.start()
     greet_across(ready)
-    load.wait()
 
     def from_block(block, c, width):
         for k in range(width // LANES):
@@ -121,43 +125,63 @@
         return stage[pl.ds(c, many, stride=SUB), :]
 
     def dispatch(step, carry):
-        start = partner(step) * group
-        slots = (lax.broadcasted_iota(jnp.int32, (many, tok), 0) + start * capacity).astype(F32)
-        pick = ((slots == prow[0:1, :]) | (slots == prow[1:2, :])).astype(BF16)
+        path = (step + side - 1) // side
+        hops = jnp.where(step == 0, 0, (step - 1) % side)
+        sign = way * (3 - 2 * path) * first(step > 0)
+        source = along(-sign) * group + q
+        target = along(sign * hops)
+
+        @pl.when(step == 1)
+        def _():
+            for copy in ahead:
+                copy.wait_recv()
+
+        @pl.when(step == side + 1)
+        def _():
+            for copy in behind:
+                copy.wait_recv()
+
+        wanted = (lax.broadcasted_iota(jnp.int32, (many, tok), 0) + target * many).astype(F32)
+        pick = ((wanted == slots_of[path, 0:1, :]) | (wanted == slots_of[path, 1:2, :])).astype(BF16)
         width = 256
         for c in range(SUB * LANES // width):
             from_block(
-                jnp.dot(pick, tokens_ref[:, c * width : (c + 1) * width], preferred_element_type=F32), c, width
+                jnp.dot(pick, near[path, :, c * width : (c + 1) * width], preferred_element_type=F32), c, width
             )
-        to_flat(outgoing, start)
+        to_flat(outgoing, step * group)
 
         def send(i, carry):
-            slot, there = member(step, i)
+            there = across(i, way)
             pltpu.make_async_remote_copy(
-                src_ref=outgoing.at[slot], dst_ref=received.at[place], send_sem=out_send,
-                recv_sem=out_recv.at[step], device_id=(there, core), device_id_type=MESH,
+                src_ref=outgoing.at[step * group + there], dst_ref=received.at[source], send_sem=out_send,
+                recv_sem=out_recv.at[step], device_id=(target * group + there, core), device_id_type=MESH,
             ).start()
             return carry
 
+        @pl.when(hops == 0)
+        def _():
+            pltpu.make_async_copy(
+                outgoing.at[step * group + q], received.at[source], out_recv.at[step]
+            ).start()
+
+        lax.fori_loop(first(hops == 0), group, send, 0)
+
         @pl.when(step == 0)
         def _():
-            pltpu.make_async_copy(outgoing.at[place], received.at[place], out_recv.at[0]).start()
-
-        lax.fori_loop(first(step), NZ, send, 0)
-
-        @pl.when(step == 0)
-        def _():
-            pl.semaphore_wait(ready, plane - 1)
-
-        lax.fori_loop(NZ, group, send, 0)
-        return carry
-
-    lax.fori_loop(0, groups, dispatch, 0)
+            pl.semaphore_wait(ready, group - 1)
+            for copy in ahead:
+                copy.wait_send()
+            for copy in behind:
+                copy.start()
+
+        return carry
+
+    lax.fori_loop(0, NZ, dispatch, 0)
     for copy in other:
         copy.start()
 
     for j in range(2):
-        pcol[j] = jnp.transpose(jnp.broadcast_to(prow[j : j + 1, :], (LANES, tok)))
+        pcol[j] = jnp.transpose(jnp.broadcast_to(slots_of[0, j : j + 1, :], (LANES, tok)))
         wcol[j] = jnp.transpose(jnp.broadcast_to(weights_ref[j : j + 1, :], (LANES, tok)))
 
     def gated(block, gate_w, up_w):
@@ -179,7 +203,7 @@
         other[i].wait()
 
     def expert(step, carry):
-        start = partner(step) * group
+        start = along(-way * offset(step)) * group
         pltpu.make_async_remote_copy(
             src_ref=outgoing.at[pl.ds(0, group)], dst_ref=received.at[pl.ds(start, group)],
             send_sem=out_send, recv_sem=out_recv.at[step], device_id=(me, 1 - core), device_id_type=MESH,
@@ -199,23 +223,23 @@
         to_flat(results, start)
 
         def send(i, carry):
-            slot, there = member(step, i)
+            there = start + across(i, -way)
             pltpu.make_async_remote_copy(
-                src_ref=results.at[slot], dst_ref=returned.at[place], send_sem=back_send,
+                src_ref=results.at[there], dst_ref=returned.at[me], send_sem=back_send,
                 recv_sem=back_recv.at[step], device_id=(there, core), device_id_type=MESH,
             ).start()
             return carry
 
         @pl.when(step == 0)
         def _():
-            pltpu.make_async_copy(results.at[place], returned.at[place], back_recv.at[0]).start()
-
-        lax.fori_loop(first(step), group, send, 0)
-        return carry
-
-    lax.fori_loop(0, groups, expert, 0)
-
-    values = tokens_ref[...].astype(F32)
+            pltpu.make_async_copy(results.at[me], returned.at[me], back_recv.at[0]).start()
+
+        lax.fori_loop(first(step == 0), group, send, 0)
+        return carry
+
+    lax.fori_loop(0, NZ, expert, 0)
+
+    values = near[0].astype(F32)
     scale = lax.rsqrt(jnp.mean(values * values, axis=1, keepdims=True) + epsilon)
     normed[...] = (values * scale * gain_ref[...]).astype(BF16)
     for i in range(3, 6):
@@ -233,11 +257,11 @@
     lax.fori_loop(0, 2, shared, 0)
 
     def combine(step, carry):
-        start = partner(step) * group
-        slots = (lax.broadcasted_iota(jnp.int32, (tok, many), 1) + start * capacity).astype(F32)
+        start = along(way * offset(step)) * group
+        wanted = (lax.broadcasted_iota(jnp.int32, (tok, many), 1) + start * capacity).astype(F32)
         share = jnp.zeros((tok, many), F32)
         for j in range(2):
-            share = share + jnp.where(slots == pcol[j, :, 0:1], wcol[j, :, 0:1], 0.0)
+            share = share + jnp.where(wanted == pcol[j, :, 0:1], wcol[j, :, 0:1], 0.0)
         high = share.astype(BF16)
         low = (share - high.astype(F32)).astype(BF16)
         pltpu.make_async_remote_copy(
@@ -254,11 +278,13 @@
             ) + jnp.dot(low, part, preferred_element_type=F32)
         return carry
 
-    lax.fori_loop(0, groups, combine, 0)
+    lax.fori_loop(0, NZ, combine, 0)
     out_ref[...] = total[...].astype(BF16)
 
+    for copy in behind:
+        copy.wait_send()
     pltpu.make_async_remote_copy(
-        src_ref=outgoing.at[pl.ds(0, experts - 1)], dst_ref=received.at[pl.ds(0, experts - 1)],
+        src_ref=outgoing.at[pl.ds(0, experts - 3)], dst_ref=received.at[pl.ds(0, experts - 3)],
         send_sem=out_send, recv_sem=out_recv.at[0], device_id=(me, 1 - core), device_id_type=MESH,
     ).wait_send()
     pltpu.make_async_remote_copy(
@@ -271,7 +297,7 @@
     tok, width = tokens.shape
     experts = eg.shape[0] * lax.axis_size("ep")
     capacity = 3 * tok * expert_ids.shape[1] // (2 * experts)
-    many = 2 * NZ * capacity
+    many = NY * NX * capacity
     half, half_shared = eg.shape[2], sg.shape[1]
     slots = pltpu.VMEM((experts, capacity * SUB, LANES), BF16)
     vmem, hbm = pl.BlockSpec(memory_space=pltpu.VMEM), pl.BlockSpec(memory_space=pltpu.HBM)
@@ -286,19 +312,19 @@
         in_specs=[hbm] + [vmem] * 3 + [hbm] * 6,
         out_specs=vmem,
         scratch_shapes=[
-            pltpu.VMEM((tok, width), BF16), pltpu.VMEM((tok, width), BF16),
+            pltpu.VMEM((3, tok, width), BF16), pltpu.VMEM((tok, width), BF16),
             slots, slots, slots, slots,
             pltpu.VMEM((many * SUB, LANES), F32),
             pltpu.VMEM((many, width), BF16),
             pltpu.VMEM((tok, width), F32),
-            pltpu.VMEM((2, tok, LANES), F32), pltpu.VMEM((2, tok, LANES), F32), pltpu.VMEM((8, tok), F32),
+            pltpu.VMEM((2, tok, LANES), F32), pltpu.VMEM((2, tok, LANES), F32), pltpu.VMEM((3, 8, tok), F32),
             pltpu.VMEM((2, width, half), BF16), pltpu.VMEM((2, width, half), BF16), pltpu.VMEM((2, half, width), BF16),
             pltpu.VMEM((2, width, half_shared), BF16), pltpu.VMEM((2, width, half_shared), BF16),
             pltpu.VMEM((2, half_shared, width), BF16),
-            dma, pltpu.SemaphoreType.REGULAR, dma((6,)), dma((6,)), dma((6,)), dma, dma((NY * NX // 2,)), dma, dma((NY * NX // 2,)),
+            dma, pltpu.SemaphoreType.REGULAR, dma((2, 2)), dma((2, 2)), dma((6,)), dma((6,)), dma((6,)), dma, dma((NZ,)), dma, dma((NZ,)),
         ],
         compiler_params=pltpu.CompilerParams(
-            collective_id=0, has_side_effects=True, vmem_limit_bytes=36 * 2**20
+            collective_id=0, has_side_effects=True, vmem_limit_bytes=40 * 2**20
         ),
         name="moe",
     )(

time: 152 us -> 150 us (0.987)
  the two profiles are of different devices: /device:TPU:1 before, /device:TPU:106 now
where the time goes in v3:
time: 150 us
  Pallas kernels  149 us (99%)
    pallas_call x1, Pallas kernels, body(): pl.pallas_call(kernel, out_shape=jax.ShapeDtypeStruct((tok, width), BF16)...  149 us

profile of v3, /device:TPU:106, one launch (start us, length us, event | category | flops | bytes accessed | tf_op | source)
XLA Modules:
  0.0 149.9 jit_solution(12440331064228630474)
XLA Ops:
  0.0 149.0 %moe.1 = bf16[256,2048]{1,0:T(8,128)(2,1)S(1)} custom-call(bf16[256,2048]{1,0:T(8,128)(2,1)} %tokens_hbm.1, f32[1,2048]{1,0:T(1,128)} %bitcast.3, s32[2,256]{1,0:T(2,128)} %bitcast.4, f32[2,256]{1,0:T(2,128)} %bitcast.5, bf16[1,2048,256]{2,1,0:T(8,128)(2,1)} %eg_ref.1, bf16[1,2048,256]{2,1,0:T(8,128)(2,1)} %eu_ref.1, bf16[1,256,2048]{2,1,0:T(8,128)(2,1)} %ed_ref.1, ...), custom_call_target="tpu_custom_call" | custom-call | tf_op jit(solution)/shard_map/moe/pallas_call | solution.py:309
  149.0 1.0 copy.12

commit v4 on v3

--- a/solution.py
+++ b/solution.py
@@ -16,8 +16,9 @@
     tokens_hbm, gain_ref, ids_ref, weights_ref, eg_ref, eu_ref, ed_ref, sg_ref, su_ref, sd_ref,
     out_ref,
     near, normed, outgoing, received, results, returned, stage, rows, total, pcol, wcol, slots_of,
+    part_out, part_in,
     wg, wu, wd, vg, vu, vd,
-    token_sem, ready, near_send, near_recv, local_sem, half_send, half_recv, out_send, out_recv, back_send, back_recv,
+    token_sem, ready, near_send, near_recv, part_send, part_recv, local_sem, half_send, half_recv, out_send, out_recv, back_send, back_recv,
 ):
     group = NY * NX
     experts = NZ * group
@@ -92,6 +93,7 @@
         slot = jnp.sum(hot * before, axis=0, keepdims=True)
         base = base + jnp.sum(hot, axis=1, keepdims=True)
         slots_of[0, j : j + 1, :] = named * capacity + slot
+        slots_of[0, 2 + j : 3 + j, :] = weights_ref[j : j + 1, :]
 
     load.wait()
     pl.semaphore_wait(barrier, NZ - 1 + group - 1 + 1)
@@ -124,10 +126,13 @@
     def column(c):
         return stage[pl.ds(c, many, stride=SUB), :]
 
-    def dispatch(step, carry):
+    def route(step):
         path = (step + side - 1) // side
         hops = jnp.where(step == 0, 0, (step - 1) % side)
-        sign = way * (3 - 2 * path) * first(step > 0)
+        return path, way * (3 - 2 * path) * first(step > 0), hops
+
+    def dispatch(step, carry):
+        path, sign, hops = route(step)
         source = along(-sign) * group + q
         target = along(sign * hops)
 
@@ -180,9 +185,11 @@
     for copy in other:
         copy.start()
 
-    for j in range(2):
-        pcol[j] = jnp.transpose(jnp.broadcast_to(slots_of[0, j : j + 1, :], (LANES, tok)))
-        wcol[j] = jnp.transpose(jnp.broadcast_to(weights_ref[j : j + 1, :], (LANES, tok)))
+    for path in range(3):
+        for j in range(2):
+            for k, ref in ((0, pcol), (2, wcol)):
+                row = slots_of[path, j + k : j + k + 1, :]
+                ref[path, j] = jnp.transpose(jnp.broadcast_to(row, (LANES, tok)))
 
     def gated(block, gate_w, up_w):
         parts = []
@@ -221,20 +228,25 @@
         for c in range(4):
             from_block(down(parts, wd, c, 512), c, 512)
         to_flat(results, start)
+        _, sign, hops = route(step)
+        target = along(-sign * hops)
 
         def send(i, carry):
-            there = start + across(i, -way)
+            there = across(i, -way)
             pltpu.make_async_remote_copy(
-                src_ref=results.at[there], dst_ref=returned.at[me], send_sem=back_send,
-                recv_sem=back_recv.at[step], device_id=(there, core), device_id_type=MESH,
+                src_ref=results.at[start + there], dst_ref=returned.at[step * group + q],
+                send_sem=back_send, recv_sem=back_recv.at[step],
+                device_id=(target * group + there, core), device_id_type=MESH,
             ).start()
             return carry
 
-        @pl.when(step == 0)
-        def _():
-            pltpu.make_async_copy(results.at[me], returned.at[me], back_recv.at[0]).start()
-
-        lax.fori_loop(first(step == 0), group, send, 0)
+        @pl.when(hops == 0)
+        def _():
+            pltpu.make_async_copy(
+                results.at[start + q], returned.at[step * group + q], back_recv.at[step]
+            ).start()
+
+        lax.fori_loop(first(hops == 0), group, send, 0)
         return carry
 
     lax.fori_loop(0, NZ, expert, 0)
@@ -251,36 +263,61 @@
         at_rows = pl.ds(pl.multiple_of(step * step_rows, step_rows), step_rows)
         parts = gated(normed[at_rows, :], vg, vu)
         for c in range(4):
-            total[at_rows, c * 512 : (c + 1) * 512] = down(parts, vd, c, 512)
+            total[0, at_rows, c * 512 : (c + 1) * 512] = down(parts, vd, c, 512)
         return carry
 
     lax.fori_loop(0, 2, shared, 0)
 
-    def combine(step, carry):
-        start = along(way * offset(step)) * group
-        wanted = (lax.broadcasted_iota(jnp.int32, (tok, many), 1) + start * capacity).astype(F32)
+    for path in range(1, 3):
+        total[path] = jnp.zeros(total.shape[1:], F32)
+
+    def summed(path):
+        there = along(-way * (1 - 2 * path)) * group + q
+        return pltpu.make_async_remote_copy(
+            src_ref=part_out.at[path], dst_ref=part_in.at[path], send_sem=part_send.at[path],
+            recv_sem=part_recv.at[path], device_id=(there, core), device_id_type=MESH,
+        )
+
+    def combine(turn, carry):
+        step = (turn + 1) % NZ
+        path, sign, hops = route(step)
+        wanted = (
+            lax.broadcasted_iota(jnp.int32, (tok, many), 1) + along(sign * hops) * many
+        ).astype(F32)
         share = jnp.zeros((tok, many), F32)
         for j in range(2):
-            share = share + jnp.where(wanted == pcol[j, :, 0:1], wcol[j, :, 0:1], 0.0)
+            share = share + jnp.where(wanted == pcol[path, j, :, 0:1], wcol[path, j, :, 0:1], 0.0)
         high = share.astype(BF16)
         low = (share - high.astype(F32)).astype(BF16)
         pltpu.make_async_remote_copy(
-            src_ref=results.at[pl.ds(0, group)], dst_ref=returned.at[pl.ds(start, group)],
+            src_ref=results.at[pl.ds(0, group)], dst_ref=returned.at[pl.ds(step * group, group)],
             send_sem=back_send, recv_sem=back_recv.at[step], device_id=(me, 1 - core), device_id_type=MESH,
         ).wait_recv()
-        from_flat(returned, start)
+        from_flat(returned, step * group)
         for c in range(SUB):
             rows[:, c * LANES : (c + 1) * LANES] = column(c).astype(BF16)
         for c in range(4):
             part = rows[:, c * 512 : (c + 1) * 512]
-            total[:, c * 512 : (c + 1) * 512] += jnp.dot(
+            total[path, :, c * 512 : (c + 1) * 512] += jnp.dot(
                 high, part, preferred_element_type=F32
             ) + jnp.dot(low, part, preferred_element_type=F32)
+
+        for path, last in ((0, side), (1, NZ - 1)):
+
+            @pl.when(step == last)
+            def _(path=path):
+                part_out[path] = total[1 + path].astype(BF16)
+                summed(path).start()
+
         return carry
 
     lax.fori_loop(0, NZ, combine, 0)
-    out_ref[...] = total[...].astype(BF16)
-
+    for path in range(2):
+        summed(path).wait_recv()
+    out_ref[...] = (total[0] + (part_in[0].astype(F32) + part_in[1].astype(F32))).astype(BF16)
+
+    for path in range(2):
+        summed(path).wait_send()
     for copy in behind:
         copy.wait_send()
     pltpu.make_async_remote_copy(
@@ -288,7 +325,7 @@
         send_sem=out_send, recv_sem=out_recv.at[0], device_id=(me, 1 - core), device_id_type=MESH,
     ).wait_send()
     pltpu.make_async_remote_copy(
-        src_ref=results.at[pl.ds(0, experts - 1)], dst_ref=returned.at[pl.ds(0, experts - 1)],
+        src_ref=results.at[pl.ds(0, experts - 3)], dst_ref=returned.at[pl.ds(0, experts - 3)],
         send_sem=back_send, recv_sem=back_recv.at[0], device_id=(me, 1 - core), device_id_type=MESH,
     ).wait_send()
 
@@ -316,15 +353,16 @@
             slots, slots, slots, slots,
             pltpu.VMEM((many * SUB, LANES), F32),
             pltpu.VMEM((many, width), BF16),
-            pltpu.VMEM((tok, width), F32),
-            pltpu.VMEM((2, tok, LANES), F32), pltpu.VMEM((2, tok, LANES), F32), pltpu.VMEM((3, 8, tok), F32),
+            pltpu.VMEM((3, tok, width), F32),
+            pltpu.VMEM((3, 2, tok, LANES), F32), pltpu.VMEM((3, 2, tok, LANES), F32), pltpu.VMEM((3, 8, tok), F32),
+            pltpu.VMEM((2, tok, width), BF16), pltpu.VMEM((2, tok, width), BF16),
             pltpu.VMEM((2, width, half), BF16), pltpu.VMEM((2, width, half), BF16), pltpu.VMEM((2, half, width), BF16),
             pltpu.VMEM((2, width, half_shared), BF16), pltpu.VMEM((2, width, half_shared), BF16),
             pltpu.VMEM((2, half_shared, width), BF16),
-            dma, pltpu.SemaphoreType.REGULAR, dma((2, 2)), dma((2, 2)), dma((6,)), dma((6,)), dma((6,)), dma, dma((NZ,)), dma, dma((NZ,)),
+            dma, pltpu.SemaphoreType.REGULAR, dma((2, 2)), dma((2, 2)), dma((2,)), dma((2,)), dma((6,)), dma((6,)), dma((6,)), dma, dma((NZ,)), dma, dma((NZ,)),
         ],
         compiler_params=pltpu.CompilerParams(
-            collective_id=0, has_side_effects=True, vmem_limit_bytes=40 * 2**20
+            collective_id=0, has_side_effects=True, vmem_limit_bytes=50 * 2**20
         ),
         name="moe",
     )(

time: 150 us -> 142 us (0.947)
  the two profiles are of different devices: /device:TPU:106 before, /device:TPU:1 now
where the time goes in v4:
time: 142 us
  Pallas kernels  141 us (99%)
    pallas_call x1, Pallas kernels, body(): pl.pallas_call(kernel, out_shape=jax.ShapeDtypeStruct((tok, width), BF16)...  141 us

profile of v4, /device:TPU:1, one launch (start us, length us, event | category | flops | bytes accessed | tf_op | source)
XLA Modules:
  0.0 142.0 jit_solution(6869020743468654837)
XLA Ops:
  0.0 141.1 %moe.1 = bf16[256,2048]{1,0:T(8,128)(2,1)S(1)} custom-call(bf16[256,2048]{1,0:T(8,128)(2,1)} %tokens_hbm.1, f32[1,2048]{1,0:T(1,128)} %bitcast.3, s32[2,256]{1,0:T(2,128)} %bitcast.4, f32[2,256]{1,0:T(2,128)} %bitcast.5, bf16[1,2048,256]{2,1,0:T(8,128)(2,1)} %eg_ref.1, bf16[1,2048,256]{2,1,0:T(8,128)(2,1)} %eu_ref.1, bf16[1,256,2048]{2,1,0:T(8,128)(2,1)} %ed_ref.1, ...), custom_call_target="tpu_custom_call" | custom-call | tf_op jit(solution)/shard_map/moe/pallas_call | solution.py:346
  141.1 1.0 copy.12

commit v5 on v4

--- a/solution.py
+++ b/solution.py
@@ -13,12 +13,12 @@
 
 
 def kernel(
-    tokens_hbm, gain_ref, ids_ref, weights_ref, eg_ref, eu_ref, ed_ref, sg_ref, su_ref, sd_ref,
+    tokens_hbm, gain_hbm, ids_hbm, weights_hbm, eg_ref, eu_ref, ed_ref, sg_ref, su_ref, sd_ref,
     out_ref,
-    near, normed, outgoing, received, results, returned, stage, rows, total, pcol, wcol, slots_of,
-    part_out, part_in,
+    near, normed, outgoing, received, results, returned, stage, rows, twice, total, pcol, wcol, slots_of,
+    part_out, part_in, gain_ref, ids_ref, weights_ref,
     wg, wu, wd, vg, vu, vd,
-    token_sem, ready, near_send, near_recv, part_send, part_recv, local_sem, half_send, half_recv, out_send, out_recv, back_send, back_recv,
+    token_sem, ready, near_send, near_recv, part_send, part_recv, small_sem, local_sem, half_send, half_recv, out_send, out_recv, back_send, back_recv,
 ):
     group = NY * NX
     experts = NZ * group
@@ -32,7 +32,12 @@
     way = 1 - 2 * core
 
     load = pltpu.make_async_copy(tokens_hbm, near.at[0], token_sem)
-    load.start()
+    small = [
+        pltpu.make_async_copy(a, b, small_sem.at[i])
+        for i, (a, b) in enumerate(((ids_hbm, ids_ref), (weights_hbm, weights_ref), (gain_hbm, gain_ref)))
+    ]
+    for copy in (*small, load):
+        copy.start()
 
     def along(distance):
         return (z + distance + NZ) % NZ
@@ -80,6 +85,9 @@
     ]
     for copy in own:
         copy.start()
+
+    for copy in small:
+        copy.wait()
 
     expert_at = lax.broadcasted_iota(jnp.int32, (experts, tok), 0).astype(F32)
     earlier = (
@@ -271,11 +279,16 @@
     for path in range(1, 3):
         total[path] = jnp.zeros(total.shape[1:], F32)
 
-    def summed(path):
+    pieces = part_send.shape[1]
+    piece = tok // pieces
+
+    def summed(path, n):
         there = along(-way * (1 - 2 * path)) * group + q
+        at_rows = pl.ds(n * piece, piece)
         return pltpu.make_async_remote_copy(
-            src_ref=part_out.at[path], dst_ref=part_in.at[path], send_sem=part_send.at[path],
-            recv_sem=part_recv.at[path], device_id=(there, core), device_id_type=MESH,
+            src_ref=part_out.at[path, at_rows], dst_ref=part_in.at[path, at_rows],
+            send_sem=part_send.at[path, n], recv_sem=part_recv.at[path, n],
+            device_id=(there, core), device_id_type=MESH,
         )
 
     def combine(turn, carry):
@@ -289,35 +302,43 @@
             share = share + jnp.where(wanted == pcol[path, j, :, 0:1], wcol[path, j, :, 0:1], 0.0)
         high = share.astype(BF16)
         low = (share - high.astype(F32)).astype(BF16)
+        both = jnp.concatenate([high, low], axis=1)
         pltpu.make_async_remote_copy(
             src_ref=results.at[pl.ds(0, group)], dst_ref=returned.at[pl.ds(step * group, group)],
             send_sem=back_send, recv_sem=back_recv.at[step], device_id=(me, 1 - core), device_id_type=MESH,
         ).wait_recv()
         from_flat(returned, step * group)
         for c in range(SUB):
-            rows[:, c * LANES : (c + 1) * LANES] = column(c).astype(BF16)
+            values = column(c).astype(BF16)
+            twice[0:many, c * LANES : (c + 1) * LANES] = values
+            twice[many:, c * LANES : (c + 1) * LANES] = values
         for c in range(4):
-            part = rows[:, c * 512 : (c + 1) * 512]
             total[path, :, c * 512 : (c + 1) * 512] += jnp.dot(
-                high, part, preferred_element_type=F32
-            ) + jnp.dot(low, part, preferred_element_type=F32)
+                both, twice[:, c * 512 : (c + 1) * 512], preferred_element_type=F32
+            )
 
         for path, last in ((0, side), (1, NZ - 1)):
 
             @pl.when(step == last)
             def _(path=path):
-                part_out[path] = total[1 + path].astype(BF16)
-                summed(path).start()
+                for n in range(pieces):
+                    at_rows = pl.ds(n * piece, piece)
+                    part_out[path, at_rows] = total[1 + path, at_rows].astype(BF16)
+                    summed(path, n).start()
 
         return carry
 
     lax.fori_loop(0, NZ, combine, 0)
-    for path in range(2):
-        summed(path).wait_recv()
-    out_ref[...] = (total[0] + (part_in[0].astype(F32) + part_in[1].astype(F32))).astype(BF16)
-
-    for path in range(2):
-        summed(path).wait_send()
+    for n in range(pieces):
+        for path in range(2):
+            summed(path, n).wait_recv()
+        at_rows = pl.ds(n * piece, piece)
+        added = part_in[0, at_rows].astype(F32) + part_in[1, at_rows].astype(F32)
+        out_ref[at_rows, :] = (total[0, at_rows] + added).astype(BF16)
+
+    for n in range(pieces):
+        for path in range(2):
+            summed(path, n).wait_send()
     for copy in behind:
         copy.wait_send()
     pltpu.make_async_remote_copy(
@@ -346,20 +367,21 @@
     return pl.pallas_call(
         kernel,
         out_shape=jax.ShapeDtypeStruct((tok, width), BF16),
-        in_specs=[hbm] + [vmem] * 3 + [hbm] * 6,
+        in_specs=[hbm] * 10,
         out_specs=vmem,
         scratch_shapes=[
             pltpu.VMEM((3, tok, width), BF16), pltpu.VMEM((tok, width), BF16),
             slots, slots, slots, slots,
             pltpu.VMEM((many * SUB, LANES), F32),
-            pltpu.VMEM((many, width), BF16),
+            pltpu.VMEM((many, width), BF16), pltpu.VMEM((2 * many, width), BF16),
             pltpu.VMEM((3, tok, width), F32),
             pltpu.VMEM((3, 2, tok, LANES), F32), pltpu.VMEM((3, 2, tok, LANES), F32), pltpu.VMEM((3, 8, tok), F32),
             pltpu.VMEM((2, tok, width), BF16), pltpu.VMEM((2, tok, width), BF16),
+            pltpu.VMEM((1, width), F32), pltpu.VMEM(expert_ids.T.shape, jnp.int32), pltpu.VMEM(route_weights.T.shape, F32),
             pltpu.VMEM((2, width, half), BF16), pltpu.VMEM((2, width, half), BF16), pltpu.VMEM((2, half, width), BF16),
             pltpu.VMEM((2, width, half_shared), BF16), pltpu.VMEM((2, width, half_shared), BF16),
             pltpu.VMEM((2, half_shared, width), BF16),
-            dma, pltpu.SemaphoreType.REGULAR, dma((2, 2)), dma((2, 2)), dma((2,)), dma((2,)), dma((6,)), dma((6,)), dma((6,)), dma, dma((NZ,)), dma, dma((NZ,)),
+            dma, pltpu.SemaphoreType.REGULAR, dma((2, 2)), dma((2, 2)), dma((2, 4)), dma((2, 4)), dma((3,)), dma((6,)), dma((6,)), dma((6,)), dma, dma((NZ,)), dma, dma((NZ,)),
         ],
         compiler_params=pltpu.CompilerParams(
             collective_id=0, has_side_effects=True, vmem_limit_bytes=50 * 2**20

time: 142 us -> 141 us (level)
  no operation moved by 1% of the time
where the time goes in v5:
time: 141 us
  Pallas kernels  140 us (99%)
    pallas_call x1, Pallas kernels, body(): pl.pallas_call(kernel, out_shape=jax.ShapeDtypeStruct((tok, width), BF16)...  140 us

profile of v5, /device:TPU:1, one launch (start us, length us, event | category | flops | bytes accessed | tf_op | source)
XLA Modules:
  0.0 140.7 jit_solution(16426888252673559721)
XLA Ops:
  0.0 139.8 %moe.1 = bf16[256,2048]{1,0:T(8,128)(2,1)S(1)} custom-call(bf16[256,2048]{1,0:T(8,128)(2,1)} %tokens_hbm.1, f32[1,2048]{1,0:T(1,128)} %bitcast.3, s32[2,256]{1,0:T(2,128)} %bitcast.4, f32[2,256]{1,0:T(2,128)} %bitcast.5, bf16[1,2048,256]{2,1,0:T(8,128)(2,1)} %eg_ref.1, bf16[1,2048,256]{2,1,0:T(8,128)(2,1)} %eu_ref.1, bf16[1,256,2048]{2,1,0:T(8,128)(2,1)} %ed_ref.1, ...), custom_call_target="tpu_custom_call" | custom-call | tf_op jit(solution)/shard_map/moe/pallas_call | solution.py:367
  139.8 1.0 copy.12

commit v6 on v5

--- a/solution.py
+++ b/solution.py
@@ -86,6 +86,23 @@
     for copy in own:
         copy.start()
 
+    load.wait()
+    pl.semaphore_wait(barrier, NZ - 1 + group - 1 + 1)
+
+    def whole(path):
+        there = along(way * (1 - 2 * path)) * group + q
+        return [
+            pltpu.make_async_remote_copy(
+                src_ref=ref.at[0], dst_ref=ref.at[1 + path], send_sem=near_send.at[path, i],
+                recv_sem=near_recv.at[path, i], device_id=(there, core), device_id_type=MESH,
+            )
+            for i, ref in enumerate((near, slots_of))
+        ]
+
+    ahead, behind = whole(0), whole(1)
+    ahead[0].start()
+    greet_across(ready)
+
     for copy in small:
         copy.wait()
 
@@ -102,24 +119,7 @@
         base = base + jnp.sum(hot, axis=1, keepdims=True)
         slots_of[0, j : j + 1, :] = named * capacity + slot
         slots_of[0, 2 + j : 3 + j, :] = weights_ref[j : j + 1, :]
-
-    load.wait()
-    pl.semaphore_wait(barrier, NZ - 1 + group - 1 + 1)
-
-    def whole(path):
-        there = along(way * (1 - 2 * path)) * group + q
-        return [
-            pltpu.make_async_remote_copy(
-                src_ref=ref.at[0], dst_ref=ref.at[1 + path], send_sem=near_send.at[path, i],
-                recv_sem=near_recv.at[path, i], device_id=(there, core), device_id_type=MESH,
-            )
-            for i, ref in enumerate((near, slots_of))
-        ]
-
-    ahead, behind = whole(0), whole(1)
-    for copy in ahead:
-        copy.start()
-    greet_across(ready)
+    ahead[1].start()
 
     def from_block(block, c, width):
         for k in range(width // LANES):

time: 141 us -> 141 us (level)
  no operation moved by 1% of the time
where the time goes in v6:
time: 141 us
  Pallas kernels  140 us (99%)
    pallas_call x1, Pallas kernels, body(): pl.pallas_call(kernel, out_shape=jax.ShapeDtypeStruct((tok, width), BF16)...  140 us

profile of v6, /device:TPU:1, one launch (start us, length us, event | category | flops | bytes accessed | tf_op | source)
XLA Modules:
  0.0 140.8 jit_solution(7632818969770832203)
XLA Ops:
  0.0 139.8 %moe.1 = bf16[256,2048]{1,0:T(8,128)(2,1)S(1)} custom-call(bf16[256,2048]{1,0:T(8,128)(2,1)} %tokens_hbm.1, f32[1,2048]{1,0:T(1,128)} %bitcast.3, s32[2,256]{1,0:T(2,128)} %bitcast.4, f32[2,256]{1,0:T(2,128)} %bitcast.5, bf16[1,2048,256]{2,1,0:T(8,128)(2,1)} %eg_ref.1, bf16[1,2048,256]{2,1,0:T(8,128)(2,1)} %eu_ref.1, bf16[1,256,2048]{2,1,0:T(8,128)(2,1)} %ed_ref.1, ...), custom_call_target="tpu_custom_call" | custom-call | tf_op jit(solution)/shard_map/moe/pallas_call | solution.py:367
  139.8 1.0 copy.12
